TPU v7x, 32 devices: a whole 2x2x4 slice. The times are simulated.
32 devices in a mesh: ep: 8 (over z, x), tp: 4 (over y, core).
Axes of the slice: x: 2, y: 2, z: 4, core: 2. Of those that a mesh axis runs over, the one named last changes fastest.
Arguments:
- tokens: bfloat16 [2048, 2048], P('ep', 'tp'), may hold values from -6 to 6
- row_ids: int32 [2048, 16], P('ep'), may hold values from 0 to 32767, as said below
- row_gates: float32 [2048, 16], P('ep'), may hold values from 0.02 to 0.5
- key_table: bfloat16 [32768, 2048], P('ep', 'tp'), may hold values from -0.125 to 0.125
- value_table: bfloat16 [32768, 2048], P('ep', 'tp'), may hold values from -14 to 14
- norm_gain: float32 [2048], P('tp'), may hold values from 0.1 to 1.9
Outputs:
- output: bfloat16 [2048, 2048], P('ep', 'tp')
Inputs may be any that keep to these rules, and one draw needn't show every extreme that they name: `row_ids`: table row r belongs to index r // 4096 of ep. The 256 tokens of one index of ep choose at most 1536 rows belonging to any one index, exactly 1536 from some index, and at least one from every index.
All inputs are finite; a program needn't handle non-finite values.
Results may differ from a plain program's by a relative error of at most 0.0065.
Values may be sent and summed in bfloat16 or wider, within the bound.
A program may use at most 64 MiB of HBM per device.

v0:
```python
import math

import jax
import jax.numpy as jnp
from jax import lax
from jax.sharding import PartitionSpec as P

D = 2048


def body(tokens, row_ids, row_gates, key_table, value_table, norm_gain):
    tok_dev, width = tokens.shape
    picks = row_ids.shape[1]
    exp_dev = key_table.shape[0]
    all_rows = lax.all_gather(tokens, "ep", axis=0, tiled=True)
    all_ids, all_gates = (
        lax.all_gather(row_ids, "ep", axis=0, tiled=True),
        lax.all_gather(row_gates, "ep", axis=0, tiled=True),
    )
    count_all = all_rows.shape[0]
    local = all_ids - lax.axis_index("ep") * exp_dev
    owned = (local >= 0) & (local < exp_dev)
    clipped = jnp.clip(local, 0, exp_dev - 1)
    block = math.gcd(count_all, 512)
    steps_all = count_all // block

    def block_scores(args):
        vectors, wanted = args
        return jnp.einsum(
            "ti,tki->tk", vectors, key_table[wanted], preferred_element_type=jnp.float32
        )

    partial_value = lax.map(
        block_scores,
        (all_rows.reshape(steps_all, block, width), clipped.reshape(steps_all, block, picks)),
    )
    partial_value = jnp.where(owned, partial_value.reshape(count_all, picks), 0.0)
    score = lax.psum(partial_value, "tp")
    hidden = jnp.where(owned, jax.nn.gelu(score, approximate=False) * all_gates, 0.0)
    count = tok_dev * lax.axis_size("ep")
    weights = lax.slice_in_dim(hidden, 0, count, axis=0)
    wanted = clipped
    inner = math.gcd(count, 512)
    turns = count // inner

    def block_terms(args):
        part_weights, part_wanted = args
        return jnp.einsum(
            "tk,tki->ti",
            part_weights,
            value_table[part_wanted].astype(jnp.float32),
            precision=lax.Precision.HIGHEST,
        )

    terms = lax.map(
        block_terms, (weights.reshape(turns, inner, picks), wanted.reshape(turns, inner, picks))
    )
    mixed = lax.psum_scatter(terms.reshape(count, width), "ep", scatter_dimension=0, tiled=True)
    squares = lax.psum(jnp.sum(mixed * mixed, axis=1), "tp")
    strength = squares / D
    return (mixed * lax.rsqrt(strength + 1e-06)[:, None] * norm_gain).astype(jnp.bfloat16)


def solution(mesh):
    in_specs = (P("ep", "tp"), P("ep", None), P("ep", None), P("ep", "tp"), P("ep", "tp"), P("tp"))
    out_specs = P("ep", "tp")
    return jax.shard_map(body, mesh=mesh, in_specs=in_specs, out_specs=out_specs, check_vma=False)
```

profile of v0, /device:TPU:0, one launch (start us, length us, event | category | flops | bytes accessed | tf_op | source)
XLA Modules:
  0.0 553.0 jit_solution(5361559708414720153)
XLA Ops:
  6.5 0.0 all-gather.2.cloned.1.call-start
  6.5 0.7 all-gather.2.cloned.1.call-update
  7.3 0.0 all-reduce.2.cloned.1.call-start
  7.3 33.0 %all_gather.9 = s32[2048,16]{0,1:T(8,128)S(1)} all-gather(s32[256,16]{0,1:T(8,128)} %param.11), channel_id=1, replica_groups=mesh['ep'=8,'tp'=4] {'ep'}, dimensions={0}, use_global_device_ids=true | all-gather | bytes 147456 | tf_op jit(solution)/shard_map/all_gather | solution.py:17
  40.4 0.3 copy.15
  40.7 21.0 %all-gather.2.cloned.1.call-done = bf16[2048,512]{1,0:T(8,128)(2,1)} async-done(((bf16[256,512]{1,0:T(8,128)(2,1)}), bf16[2048,512]{1,0:T(8,128)(2,1)}) %all-gather.2.cloned.1.call-update) | async-done | bytes 2097168 | tf_op jit(solution)/shard_map/all_gather | solution.py:15
  61.7 177.4 %while.20 = (s32[]{:T(128)}, f32[4,512,16]{1,0,2:T(4,128)S(1)}, bf16[4,512,512]{2,1,0:T(8,128)(2,1)}, s32[4,512,16]{2,1,0:T(8,128)S(1)}, bf16[4096,512]{1,0:T(8,128)(2,1)}, /*index=5*/s32[]{:T(128)}, s32[]{:T(128)}) while((s32[]{:T(128)}, f32[4,512,16]{1,0,2:T(4,128)S(1)}, bf16[4,512,512]{2,1,0:T(8,128)(2,1)}, s32[4,512,16]{2,1,0:T(8,128)S(1)}, ...), condition=%wide.region_1.2_spmd, body=%wide.region_0.1_spmd.sunk | while | flops 8421378 | bytes 27197528 | solution.py:33
  61.7 0.1 reshape.109
  61.9 36.7 %gather_fusion = bf16[8192,512]{1,0:T(8,128)(2,1)} fusion(bf16[4096,512]{1,0:T(8,128)(2,1)} %get-tuple-element.173, s32[8192]{0:T(1024)S(1)} %broadcast_clamp_fusion.4), kind=kCustom, calls=%fused_computation.clone.1 | custom fusion | bytes 16809984 | tf_op jit(solution)/shard_map/while/body/eval_jaxpr/gather | solution.py:30
  98.6 1.1 dynamic-slice_bitcast_fusion.2
  99.6 6.0 %fusion.25 = f32[512,1,16]{2,1,0:T(1,128)S(1)} fusion(bf16[512,16,512]{2,1,0:T(8,128)(2,1)} %bitcast.57, bf16[512,512,1]{1,0,2:T(8,128)(2,1)S(1)} %dynamic-slice_bitcast_fusion.2), kind=kOutput, calls=%fused_computation.2.clone.1 | convolution fusion | flops 8388608 | bytes 8945664 | tf_op jit(solution)/shard_map/while/body/eval_jaxpr/ti,tki->tk/dot_general | solution.py:29
  105.7 0.1 copy.33
  105.8 0.2 dynamic_update_slice.11
  106.1 0.1 reshape.109
  106.2 36.7 %gather_fusion = bf16[8192,512]{1,0:T(8,128)(2,1)} fusion(bf16[4096,512]{1,0:T(8,128)(2,1)} %get-tuple-element.173, s32[8192]{0:T(1024)S(1)} %broadcast_clamp_fusion.4), kind=kCustom, calls=%fused_computation.clone.1 | custom fusion | bytes 16809984 | tf_op jit(solution)/shard_map/while/body/eval_jaxpr/gather | solution.py:30
  142.9 1.1 dynamic-slice_bitcast_fusion.2
  144.0 6.0 %fusion.25 = f32[512,1,16]{2,1,0:T(1,128)S(1)} fusion(bf16[512,16,512]{2,1,0:T(8,128)(2,1)} %bitcast.57, bf16[512,512,1]{1,0,2:T(8,128)(2,1)S(1)} %dynamic-slice_bitcast_fusion.2), kind=kOutput, calls=%fused_computation.2.clone.1 | convolution fusion | flops 8388608 | bytes 8945664 | tf_op jit(solution)/shard_map/while/body/eval_jaxpr/ti,tki->tk/dot_general | solution.py:29
  150.0 0.1 copy.33
  150.2 0.2 dynamic_update_slice.11
  150.4 0.1 reshape.109
  150.6 36.7 %gather_fusion = bf16[8192,512]{1,0:T(8,128)(2,1)} fusion(bf16[4096,512]{1,0:T(8,128)(2,1)} %get-tuple-element.173, s32[8192]{0:T(1024)S(1)} %broadcast_clamp_fusion.4), kind=kCustom, calls=%fused_computation.clone.1 | custom fusion | bytes 16809984 | tf_op jit(solution)/shard_map/while/body/eval_jaxpr/gather | solution.py:30
  187.3 1.1 dynamic-slice_bitcast_fusion.2
  188.3 6.0 %fusion.25 = f32[512,1,16]{2,1,0:T(1,128)S(1)} fusion(bf16[512,16,512]{2,1,0:T(8,128)(2,1)} %bitcast.57, bf16[512,512,1]{1,0,2:T(8,128)(2,1)S(1)} %dynamic-slice_bitcast_fusion.2), kind=kOutput, calls=%fused_computation.2.clone.1 | convolution fusion | flops 8388608 | bytes 8945664 | tf_op jit(solution)/shard_map/while/body/eval_jaxpr/ti,tki->tk/dot_general | solution.py:29
  194.4 0.1 copy.33
  194.5 0.2 dynamic_update_slice.11
  194.8 0.1 reshape.109
  194.9 36.7 %gather_fusion = bf16[8192,512]{1,0:T(8,128)(2,1)} fusion(bf16[4096,512]{1,0:T(8,128)(2,1)} %get-tuple-element.173, s32[8192]{0:T(1024)S(1)} %broadcast_clamp_fusion.4), kind=kCustom, calls=%fused_computation.clone.1 | custom fusion | bytes 16809984 | tf_op jit(solution)/shard_map/while/body/eval_jaxpr/gather | solution.py:30
  231.6 1.1 dynamic-slice_bitcast_fusion.2
  232.7 6.0 %fusion.25 = f32[512,1,16]{2,1,0:T(1,128)S(1)} fusion(bf16[512,16,512]{2,1,0:T(8,128)(2,1)} %bitcast.57, bf16[512,512,1]{1,0,2:T(8,128)(2,1)S(1)} %dynamic-slice_bitcast_fusion.2), kind=kOutput, calls=%fused_computation.2.clone.1 | convolution fusion | flops 8388608 | bytes 8945664 | tf_op jit(solution)/shard_map/while/body/eval_jaxpr/ti,tki->tk/dot_general | solution.py:29
  238.7 0.1 copy.33
  238.9 0.2 dynamic_update_slice.11
  239.1 0.7 broadcast_select_fusion
  239.8 0.0 all-reduce.2.cloned.1.call-update
  239.8 0.0 reduce-scatter.2.cloned.1.call-start
  239.9 30.6 %all_gather.11 = f32[2048,16]{0,1:T(8,128)S(1)} all-gather(f32[256,16]{0,1:T(8,128)S(1)} %copy-done), channel_id=1, replica_groups=mesh['ep'=8,'tp'=4] {'ep'}, dimensions={0}, use_global_device_ids=true | all-gather | bytes 147456 | tf_op jit(solution)/shard_map/all_gather | solution.py:18
  270.5 1.2 fusion.5
  271.7 0.1 reshape.77
  271.8 0.0 copy-start.1
  271.8 177.1 %while.21 = (s32[]{:T(128)}, f32[4,512,512]{2,1,0:T(8,128)}, f32[4,512,16]{1,0,2:T(4,128)S(1)}, s32[4,512,16]{2,1,0:T(8,128)S(1)}, bf16[4096,512]{1,0:T(8,128)(2,1)}, /*index=5*/s32[]{:T(128)}) while((s32[]{:T(128)}, f32[4,512,512]{2,1,0:T(8,128)}, f32[4,512,16]{1,0,2:T(4,128)S(1)}, s32[4,512,16]{2,1,0:T(8,128)S(1)}, ...), condition=%wide.region_4.5_spmd, body=%wide.region_3.4_spmd.sunk | while | flops 50364416 | bytes 28770892 | solution.py:55
  271.9 0.1 reshape.112
  272.0 36.7 %gather_fusion.1 = bf16[8192,512]{1,0:T(8,128)(2,1)} fusion(bf16[4096,512]{1,0:T(8,128)(2,1)} %get-tuple-element.192, s32[8192]{0:T(1024)S(1)} %broadcast_clamp_fusion.5), kind=kCustom, calls=%fused_computation.1.clone.1 | custom fusion | bytes 16809984 | tf_op jit(solution)/shard_map/while/body/eval_jaxpr/gather | solution.py:51
  308.7 0.1 copy.37
  308.9 6.2 %fusion.28 = f32[512,1,512]{2,1,0:T(1,128)S(1)} fusion(f32[512,16,1]{1,2,0:T(1,128)S(1)} %copy.37, bf16[512,16,512]{2,1,0:T(8,128)(2,1)} %bitcast.56), kind=kOutput, calls=%fused_computation.38.clone.1 | convolution fusion | flops 50331648 | bytes 9469952 | tf_op jit(solution)/shard_map/while/body/eval_jaxpr/tk,tki->ti/dot_general | solution.py:48
  315.0 1.1 bitcast_dynamic-update-slice_fusion.2
  316.2 0.1 reshape.112
  316.4 36.7 %gather_fusion.1 = bf16[8192,512]{1,0:T(8,128)(2,1)} fusion(bf16[4096,512]{1,0:T(8,128)(2,1)} %get-tuple-element.192, s32[8192]{0:T(1024)S(1)} %broadcast_clamp_fusion.5), kind=kCustom, calls=%fused_computation.1.clone.1 | custom fusion | bytes 16809984 | tf_op jit(solution)/shard_map/while/body/eval_jaxpr/gather | solution.py:51
  353.1 0.1 copy.37
  353.2 6.2 %fusion.28 = f32[512,1,512]{2,1,0:T(1,128)S(1)} fusion(f32[512,16,1]{1,2,0:T(1,128)S(1)} %copy.37, bf16[512,16,512]{2,1,0:T(8,128)(2,1)} %bitcast.56), kind=kOutput, calls=%fused_computation.38.clone.1 | convolution fusion | flops 50331648 | bytes 9469952 | tf_op jit(solution)/shard_map/while/body/eval_jaxpr/tk,tki->ti/dot_general | solution.py:48
  359.4 1.0 bitcast_dynamic-update-slice_fusion.2
  360.4 0.1 reshape.112
  360.6 36.7 %gather_fusion.1 = bf16[8192,512]{1,0:T(8,128)(2,1)} fusion(bf16[4096,512]{1,0:T(8,128)(2,1)} %get-tuple-element.192, s32[8192]{0:T(1024)S(1)} %broadcast_clamp_fusion.5), kind=kCustom, calls=%fused_computation.1.clone.1 | custom fusion | bytes 16809984 | tf_op jit(solution)/shard_map/while/body/eval_jaxpr/gather | solution.py:51
  397.3 0.1 copy.37
  397.5 6.2 %fusion.28 = f32[512,1,512]{2,1,0:T(1,128)S(1)} fusion(f32[512,16,1]{1,2,0:T(1,128)S(1)} %copy.37, bf16[512,16,512]{2,1,0:T(8,128)(2,1)} %bitcast.56), kind=kOutput, calls=%fused_computation.38.clone.1 | convolution fusion | flops 50331648 | bytes 9469952 | tf_op jit(solution)/shard_map/while/body/eval_jaxpr/tk,tki->ti/dot_general | solution.py:48
  403.6 1.0 bitcast_dynamic-update-slice_fusion.2
  404.7 0.1 reshape.112
  404.9 36.7 %gather_fusion.1 = bf16[8192,512]{1,0:T(8,128)(2,1)} fusion(bf16[4096,512]{1,0:T(8,128)(2,1)} %get-tuple-element.192, s32[8192]{0:T(1024)S(1)} %broadcast_clamp_fusion.5), kind=kCustom, calls=%fused_computation.1.clone.1 | custom fusion | bytes 16809984 | tf_op jit(solution)/shard_map/while/body/eval_jaxpr/gather | solution.py:51
  441.6 0.1 copy.37
  441.7 6.2 %fusion.28 = f32[512,1,512]{2,1,0:T(1,128)S(1)} fusion(f32[512,16,1]{1,2,0:T(1,128)S(1)} %copy.37, bf16[512,16,512]{2,1,0:T(8,128)(2,1)} %bitcast.56), kind=kOutput, calls=%fused_computation.38.clone.1 | convolution fusion | flops 50331648 | bytes 9469952 | tf_op jit(solution)/shard_map/while/body/eval_jaxpr/tk,tki->ti/dot_general | solution.py:48
  447.9 1.0 bitcast_dynamic-update-slice_fusion.2
  448.9 0.0 reduce-scatter.2.cloned.1.call-update
  449.0 88.3 %reduce-scatter.2.cloned.1.call-done = f32[256,512]{1,0:T(8,128)} async-done(((f32[2048,512]{1,0:T(8,128)}), f32[256,512]{1,0:T(8,128)}) %reduce-scatter.2.cloned.1.call-update) | async-done | bytes 524304 | tf_op jit(solution)/shard_map/reduce_scatter | solution.py:58
  537.2 1.2 multiply_reduce_fusion
  538.4 6.2 %psum.15 = f32[256]{0:T(256)S(1)} all-reduce(f32[256]{0:T(256)S(1)} %multiply_reduce_fusion), channel_id=1, replica_groups=mesh['ep'=8,'tp'=4] {'tp'}, use_global_device_ids=true, to_apply=%region_7.8 | all-reduce | flops 256 | bytes 2048 | tf_op jit(solution)/shard_map/psum | solution.py:59
  544.6 1.9 multiply_convert_fusion
  (37 shorter events, 0.7 us)
Async XLA Ops:
  6.5 55.2 %all-gather.2.cloned.1.call-start = ((), (), s32[]{:S(2)}) async-start(), calls=%async_computation.1 | async-start | bytes 2359296 | tf_op jit(solution)/shard_map/all_gather | solution.py:15
  7.3 263.2 %all-reduce.2.cloned.1.call-start = ((), (), s32[]{:S(2)}) async-start(), calls=%async_computation.2 | async-start | bytes 262144 | tf_op jit(solution)/shard_map/psum | solution.py:38
  61.7 178.2 %copy-start = (f32[256,16]{0,1:T(8,128)S(1)}, f32[256,16]{0,1:T(8,128)}, u32[]{:S(2)}) copy-start(f32[256,16]{0,1:T(8,128)} %param.12) | copy-start | bytes 49156
  239.8 297.4 %reduce-scatter.2.cloned.1.call-start = ((), (), s32[]{:S(2)}) async-start(), calls=%async_computation.3 | async-start | bytes 4718592 | tf_op jit(solution)/shard_map/reduce_scatter | solution.py:58
  271.8 272.8 %copy-start.1 = (f32[512]{0:T(512)S(1)}, f32[512]{0:T(512)}, u32[]{:S(2)}) copy-start(f32[512]{0:T(512)} %param.15) | copy-start | bytes 6148
Sparse Core Ops, SparseCore 0:
  9.5 52.1 all-gather.1
  240.0 30.2 all-reduce.1
  449.1 88.1 reduce-scatter.1
where the time goes:
time: 554 us; the launch traced here: 553 us
  local copies, waits for them, and re-layouts  305 us (55%)
  waiting for transfers between devices  110 us (20%)
  blocking collectives  69.8 us (13%)
  matrix products  48.8 us (9%)
  between operations  13.2 us (2%)
    gather x4, local copies, waits for them, and re-layouts, block_scores(): key_table[wanted]  147 us
    gather x4, local copies, waits for them, and re-layouts, block_terms(): value_table[part_wanted].astype(jnp.float32)  147 us
    reduce_scatter x1, waiting for transfers between devices, body(): lax.psum_scatter(terms.reshape(count, width), 'ep', scatter_dimension=0,...  88.3 us
    all_gather x1, blocking collectives, body(): lax.all_gather(row_ids, 'ep', axis=0, tiled=True)  33 us
    all_gather x1, blocking collectives, body(): lax.all_gather(row_gates, 'ep', axis=0, tiled=True)  30.6 us
    dot_general x4, matrix products, block_terms(): jnp.einsum('tk,tki->ti', part_weights, value_table[part_wanted].astype(jn...  24.6 us
    dot_general x4, matrix products, block_scores(): jnp.einsum('ti,tki->tk', vectors, key_table[wanted], preferred_element_ty...  24.2 us
    all_gather x1, waiting for transfers between devices, body(): all_rows = lax.all_gather(tokens, 'ep', axis=0, tiled=True)  21 us
  transfers between devices with their start and end apart: 3, of which 2 were waited for; matrix products, arithmetic and copies ran while one was open for 0% of the time, Pallas kernels for 0%

commit v1 on v0

v1 whole, which is shorter than its diff:
```python
import functools

import jax
import jax.numpy as jnp
from jax import lax
from jax.experimental import pallas as pl
from jax.experimental.pallas import tpu as pltpu
from jax.sharding import PartitionSpec as P

ROW = 256
LANES = 128
MESH = pl.DeviceIdType.MESH


def cycle_of(n):
    x = 1
    while 4 * x * x <= n:
        x *= 2
    z = n // x
    if x == 1 or z % 2:
        return list(range(n))
    out = []
    for row in range(z):
        cols = range(1, x) if row % 2 == 0 else range(x - 1, 0, -1)
        out += [row * x + col for col in cols]
    return out + [row * x for row in range(z - 1, -1, -1)]


def look(table, i):
    n = len(table)
    total = 0
    for k, v in enumerate(table):
        total = total + v * ((n * n - (i - k) * (i - k)) // (n * n))
    return total


def greet(n, tps, me, order):
    pos = look([order.index(i) for i in range(n)], me)
    right = look(order, lax.rem(pos + 1, n))
    left = look(order, lax.rem(pos + n - 1, n))
    mine = lax.axis_index("tp")
    barrier = pltpu.get_barrier_semaphore()
    for peer in (left, right):
        pl.semaphore_signal(barrier, inc=1, device_id=(peer, mine), device_id_type=MESH)
    for k in range(1, tps):
        pl.semaphore_signal(
            barrier, inc=1, device_id=(me, lax.rem(mine + k, tps)), device_id_type=MESH
        )
    pl.semaphore_wait(barrier, 2 + tps - 1)
    return pos, right, left, mine


def remote(src, dst, send, recv, device):
    return pltpu.make_async_remote_copy(
        src_ref=src, dst_ref=dst, send_sem=send, recv_sem=recv, device_id=device, device_id_type=MESH
    )


def score_kernel(n, tps, picks, order, chunks, *refs):
    x_ref, meta_ref, key_ref, hid_ref, meta_out, xall, s_ref, part, got_ref = refs[:9]
    xs, xr, ms, mr, ps, pr = refs[9:]
    block, width = x_ref.shape
    half = block // 2
    experts = key_ref.shape[0]
    rows = half // chunks
    me = lax.axis_index("ep")
    pos, right, left, mine = greet(n, tps, me, order)
    base = me * experts
    peers = (right, left)

    def x_copy(d, src_block, step, c, first):
        at = pl.ds(d * half + c * rows, rows)
        src = x_ref.at[at] if first else xall.at[src_block, at]
        return remote(
            src, xall.at[src_block, at], xs.at[d, step, c], xr.at[d, step, c], (peers[d], mine)
        )

    def m_copy(d, src_block, step, first):
        src = meta_ref.at[d] if first else meta_out.at[src_block, d]
        return remote(src, meta_out.at[src_block, d], ms.at[d, step], mr.at[d, step], (peers[d], mine))

    for d in (0, 1):
        m_copy(d, me, 0, True).start()
        for c in range(chunks):
            x_copy(d, me, 0, c, True).start()
    xall[me] = x_ref[...]
    meta_out[me] = meta_ref[...]

    per_half = LANES // picks
    sub = lax.broadcasted_iota(jnp.int32, (per_half, LANES), 0)
    lane = lax.broadcasted_iota(jnp.int32, (per_half, LANES), 1)
    own_lane = sub == lane // picks
    wide = min(512, experts)

    def step(s, carry):
        blocks = (look(order, lax.rem(pos + n - s, n)), look(order, lax.rem(pos + s, n)))

        @pl.when(s >= 1)
        def _():
            for d in (0, 1):
                m_copy(d, blocks[d], s - 1, False).wait_recv()

                @pl.when(s < n - 1)
                def _():
                    m_copy(d, blocks[d], s, False).start()

            for c in range(chunks):
                for d in (0, 1):
                    x_copy(d, blocks[d], s - 1, c, False).wait_recv()

                    @pl.when(s < n - 1)
                    def _():
                        x_copy(d, blocks[d], s, c, False).start()

        x = jnp.concatenate([xall[blocks[0], :half, :], xall[blocks[1], half:, :]], axis=0)
        for c in range(experts // wide):
            s_ref[:, c * wide : (c + 1) * wide] = lax.dot_general(
                x,
                key_ref[c * wide : (c + 1) * wide, :],
                (((1,), (1,)), ((), ())),
                preferred_element_type=jnp.float32,
            )
        for d in (0, 1):
            all_ids = meta_out[blocks[d], d, :8, :].astype(jnp.int32) - base
            for h2 in range(ROW // LANES):
                out = []
                for r in range(8):
                    ids = all_ids[r : r + 1, h2 * LANES : (h2 + 1) * LANES]
                    ids = jnp.broadcast_to(ids, (per_half, LANES))
                    owned = (ids >= 0) & (ids < experts)
                    hi = jnp.where(owned, ids >> 7, -1)
                    lo = jnp.where(owned, ids & (LANES - 1), 0)
                    row = d * half + r * (ROW // picks) + h2 * per_half
                    acc = jnp.zeros((per_half, LANES), jnp.float32)
                    for h in range(experts // LANES):
                        tile = s_ref[row : row + per_half, h * LANES : (h + 1) * LANES]
                        acc = jnp.where(hi == h, jnp.take_along_axis(tile, lo, axis=1), acc)
                    out.append(jnp.sum(jnp.where(own_lane, acc, 0.0), axis=0, keepdims=True))
                at = pl.multiple_of(blocks[d] * 16 + d * 8, 8)
                part[pl.ds(at, 8), h2 * LANES : (h2 + 1) * LANES] = jnp.concatenate(out, axis=0)
        return carry

    lax.fori_loop(0, n, step, 0)

    def p_copy(k):
        return remote(
            part, got_ref.at[k - 1], ps.at[k - 1], pr.at[k - 1], (me, lax.rem(mine + k, tps))
        )

    for k in range(1, tps):
        p_copy(k).start()

    def drain(s, carry):
        for d in (0, 1):
            m_copy(d, me, s, False).wait_send()
            for c in range(chunks):
                x_copy(d, me, s, c, False).wait_send()
        return carry

    lax.fori_loop(0, n - 1, drain, 0)
    for k in range(1, tps):
        p_copy(k).wait()
    total = part[...]
    for k in range(1, tps):
        total = total + got_ref[k - 1]
    hid_ref[...] = 0.5 * total * (1.0 + lax.erf(total * (0.5**0.5)))


def mix_kernel(n, tps, picks, order, *refs):
    h_ref, meta_ref, value_ref, gain_ref, out_ref, w_ref, sent, came, sq_ref, sq_got = refs[:10]
    ss, sr, qs, qr, out_total = refs[10:]
    experts, width = value_ref.shape
    block = out_ref.shape[0]
    half = block // 2
    me = lax.axis_index("ep")
    pos, right, left, mine = greet(n, tps, me, order)
    base = me * experts
    peers = (right, left)
    per = ROW // picks
    tall = experts // ROW * per
    lane_token = lax.broadcasted_iota(jnp.int32, (8, ROW), 1) // picks
    tall_iota = lax.broadcasted_iota(jnp.int32, (tall, ROW), 0)
    lo_iota = lax.broadcasted_iota(jnp.int32, (ROW, ROW), 0)

    def copy(d, s):
        return remote(sent.at[s, d], came.at[s, d], ss.at[d, s], sr.at[d, s], (peers[d], mine))

    def terms(s):
        blocks = (
            look(order, lax.rem(pos + 2 * n - 1 - s, n)),
            look(order, lax.rem(pos + 1 + s, n)),
        )
        for d in (0, 1):
            ids = meta_ref[blocks[d], d, :8, :].astype(jnp.int32) - base
            owned = (ids >= 0) & (ids < experts)
            codes = jnp.where(owned, (ids >> 8) * per + lane_token, -1)
            los = ids & (ROW - 1)
            at = pl.multiple_of(blocks[d] * 16 + d * 8, 8)
            hs = h_ref[pl.ds(at, 8), :] * meta_ref[blocks[d], d, 8:, :]
            for r in range(8):
                code, lo, h = codes[r : r + 1, :], los[r : r + 1, :], hs[r : r + 1, :]
                a = jnp.where(tall_iota == code, h, 0.0).astype(jnp.bfloat16)
                b = jnp.where(lo_iota == lo, 1.0, 0.0).astype(jnp.bfloat16)
                w = lax.dot_general(
                    a, b, (((1,), (1,)), ((), ())), preferred_element_type=jnp.float32
                ).astype(jnp.bfloat16)
                row = d * half + r * per
                for c in range(experts // ROW):
                    w_ref[row : row + per, c * ROW : (c + 1) * ROW] = w[c * per : (c + 1) * per, :]
        return jnp.dot(w_ref[...], value_ref[...], preferred_element_type=jnp.float32)

    def step(s, carry):
        out_total[...] = terms(s)
        for d in (0, 1):
            at = slice(d * half, (d + 1) * half)

            @pl.when(s >= 1)
            def _():
                copy(d, s - 1).wait_recv()
                out_total[at, :] = out_total[at, :] + came[s - 1, d].astype(jnp.float32)

            @pl.when(s < n - 1)
            def _():
                sent[s, d] = out_total[at, :].astype(jnp.bfloat16)
                copy(d, s).start()

        return carry

    lax.fori_loop(0, n, step, 0)
    mixed = out_total[...]
    ones = jnp.ones((8, width), jnp.float32)
    square = lax.dot_general(
        ones,
        mixed * mixed,
        (((1,), (1,)), ((), ())),
        precision=lax.Precision.HIGHEST,
        preferred_element_type=jnp.float32,
    )
    sq_ref[...] = square

    def q_copy(k):
        return remote(
            sq_ref, sq_got.at[k - 1], qs.at[k - 1], qr.at[k - 1], (me, lax.rem(mine + k, tps))
        )

    for k in range(1, tps):
        q_copy(k).start()

    def drain(s, carry):
        for d in (0, 1):
            copy(d, s).wait_send()
        return carry

    lax.fori_loop(0, n - 1, drain, 0)
    for k in range(1, tps):
        q_copy(k).wait()
    total = square
    for k in range(1, tps):
        total = total + sq_got[k - 1]
    scale = lax.rsqrt(total / (width * tps) + 1e-06)
    column = lax.dot_general(
        scale,
        jnp.full((8, LANES), 0.125, jnp.float32),
        (((0,), (0,)), ((), ())),
        precision=lax.Precision.HIGHEST,
        preferred_element_type=jnp.float32,
    )
    for c in range(width // LANES):
        at = slice(c * LANES, (c + 1) * LANES)
        out_ref[:, at] = (out_total[:, at] * column * gain_ref[:, at]).astype(jnp.bfloat16)


def body(tokens, row_ids, row_gates, key_table, value_table, norm_gain):
    block, width = tokens.shape
    picks = row_ids.shape[1]
    experts = key_table.shape[0]
    n, tps = lax.axis_size("ep"), lax.axis_size("tp")
    order = cycle_of(n)
    half = block // 2
    chunks = 2
    lines = half * picks // ROW
    meta = jnp.concatenate(
        [
            row_ids.astype(jnp.float32).reshape(2, lines, ROW),
            row_gates.reshape(2, lines, ROW),
        ],
        axis=1,
    )
    whole = pl.BlockSpec(memory_space=pltpu.VMEM)
    dma = pltpu.SemaphoreType.DMA
    hidden, metas = pl.pallas_call(
        functools.partial(score_kernel, n, tps, picks, order, chunks),
        out_shape=(
            jax.ShapeDtypeStruct((n * 2 * lines, ROW), jnp.float32),
            jax.ShapeDtypeStruct((n, 2, 2 * lines, ROW), jnp.float32),
        ),
        in_specs=[whole] * 3,
        out_specs=(whole, whole),
        scratch_shapes=[
            pltpu.VMEM((n, block, width), jnp.bfloat16),
            pltpu.VMEM((block, experts), jnp.float32),
            pltpu.VMEM((n * 2 * lines, ROW), jnp.float32),
            pltpu.VMEM((tps - 1, n * 2 * lines, ROW), jnp.float32),
            dma((2, n, chunks)),
            dma((2, n, chunks)),
            dma((2, n)),
            dma((2, n)),
            dma((tps - 1,)),
            dma((tps - 1,)),
        ],
        compiler_params=pltpu.CompilerParams(collective_id=0, has_side_effects=True),
    )(tokens, meta, key_table)
    return pl.pallas_call(
        functools.partial(mix_kernel, n, tps, picks, order),
        out_shape=jax.ShapeDtypeStruct((block, width), jnp.bfloat16),
        in_specs=[whole] * 4,
        out_specs=whole,
        scratch_shapes=[
            pltpu.VMEM((block, experts), jnp.bfloat16),
            pltpu.VMEM((n, 2, half, width), jnp.bfloat16),
            pltpu.VMEM((n, 2, half, width), jnp.bfloat16),
            pltpu.VMEM((8, block), jnp.float32),
            pltpu.VMEM((tps - 1, 8, block), jnp.float32),
            dma((2, n)),
            dma((2, n)),
            dma((tps - 1,)),
            dma((tps - 1,)),
            pltpu.VMEM((block, width), jnp.float32),
        ],
        compiler_params=pltpu.CompilerParams(collective_id=1, has_side_effects=True),
    )(hidden, metas, value_table, norm_gain.reshape(1, -1))


def solution(mesh):
    in_specs = (P("ep", "tp"), P("ep", None), P("ep", None), P("ep", "tp"), P("ep", "tp"), P("tp"))
    out_specs = P("ep", "tp")
    return jax.shard_map(body, mesh=mesh, in_specs=in_specs, out_specs=out_specs, check_vma=False)
```

time: 554 us -> 90.5 us (0.16)
  local copies, waits for them, and re-layouts: 305 us -> 2.81 us
  waiting for transfers between devices: 110 us -> 0 us
  Pallas kernels: 0 us -> 86 us
  blocking collectives: 69.8 us -> 0 us
  matrix products: 48.8 us -> 0 us
  between operations: 13.2 us -> 0.02 us
    gather x8 -> x0, local copies, waits for them, and re-layouts: 294 us -> none  [the longest x4 147 us: block_scores(): key_table[wanted]]
    reduce_scatter x1 -> x0, waiting for transfers between devices: 88.3 us -> none  [body(): lax.psum_scatter(terms.reshape(count, width), 'ep', scatter_dimension=0,...]
    pallas_call x0 -> x2, Pallas kernels: none -> 86 us  [the longest x1 43.4 us: body(): pl.pallas_call(functools.partial(score_kernel, n, tps, picks, order, chun...]
    all_gather x2 -> x0, blocking collectives: 63.6 us -> none  [the longest x1 33 us: body(): lax.all_gather(row_ids, 'ep', axis=0, tiled=True)]
    dot_general x8 -> x0, matrix products: 48.8 us -> none  [the longest x4 24.6 us: block_terms(): jnp.einsum('tk,tki->ti', part_weights, value_table[part_wanted].astype(jn...]
    all_gather x1 -> x0, waiting for transfers between devices: 21 us -> none  [body(): all_rows = lax.all_gather(tokens, 'ep', axis=0, tiled=True)]
    psum x1 -> x0, blocking collectives: 6.2 us -> none  [body(): squares = lax.psum(jnp.sum(mixed * mixed, axis=1), 'tp')]
  transfers between devices with their start and end apart: 3 -> 0, of which waited for: 2 -> 0; matrix products, arithmetic and copies ran while one was open for 0% -> 0% of each run, Pallas kernels for 0% -> 0%
where the time goes in v1:
time: 90.5 us; the launch traced here: 90.1 us
  Pallas kernels  86 us (95%)
  local copies, waits for them, and re-layouts  2.81 us (3%)
  other arithmetic  1.34 us (1%)
    pallas_call x1, Pallas kernels, body(): pl.pallas_call(functools.partial(score_kernel, n, tps, picks, order, chun...  43.4 us
    pallas_call x1, Pallas kernels, body(): pl.pallas_call(functools.partial(mix_kernel, n, tps, picks, order), out_s...  42.6 us
    unnamed x2, local copies, waits for them, and re-layouts  2.49 us

profile of v1, /device:TPU:0, one launch (start us, length us, event | category | flops | bytes accessed | tf_op | source)
XLA Modules:
  0.0 90.1 jit_solution(4594281597622488610)
XLA Ops:
  0.0 0.7 convert_element_type.3
  0.7 0.1 copy.9
  0.8 0.1 reshape.9
  0.9 0.8 copy.10
  1.8 0.1 reshape.10
  1.9 0.6 pad_maximum_fusion.refs_1_
  2.5 43.4 %shard_map.64 = (f32[128,256]{1,0:T(8,128)}, f32[8,2,16,256]{3,2,1,0:T(8,128)}) custom-call(bf16[256,512]{1,0:T(8,128)(2,1)} %refs_0_.1, f32[2,16,256]{2,1,0:T(8,128)} %pad_maximum_fusion.refs_1_, bf16[4096,512]{1,0:T(8,128)(2,1)} %refs_2_.2), custom_call_target="tpu_custom_call" | custom-call | tf_op jit(solution)/shard_map/pallas_call | solution.py:291
  45.9 42.6 %shard_map.65 = bf16[256,512]{1,0:T(8,128)(2,1)} custom-call(f32[128,256]{1,0:T(8,128)} %get-tuple-element.7.refs_0_, f32[8,2,16,256]{3,2,1,0:T(8,128)} %get-tuple-element.8.refs_1_, bf16[4096,512]{1,0:T(8,128)(2,1)} %refs_2_.3, f32[1,512]{1,0:T(1,128)} %bitcast.1), custom_call_target="tpu_custom_call" | custom-call | tf_op jit(solution)/shard_map/pallas_call | solution.py:313
  88.5 1.7 %copy.12 = bf16[256,512]{1,0:T(8,128)(2,1)} copy(bf16[256,512]{1,0:T(8,128)(2,1)} %shard_map.65) | data formatting | bytes 524288

commit v2 on v1

v2 whole, which is shorter than its diff:
```python
import functools

import jax
import jax.numpy as jnp
from jax import lax
from jax.experimental import pallas as pl
from jax.experimental.pallas import tpu as pltpu
from jax.sharding import PartitionSpec as P

ROW = 256
LANES = 128
MESH = pl.DeviceIdType.MESH


def cycle_of(n):
    x = 1
    while 4 * x * x <= n:
        x *= 2
    z = n // x
    if x == 1 or z % 2:
        return list(range(n))
    out = []
    for row in range(z):
        cols = range(1, x) if row % 2 == 0 else range(x - 1, 0, -1)
        out += [row * x + col for col in cols]
    return out + [row * x for row in range(z - 1, -1, -1)]


def look(table, i):
    n = len(table)
    total = 0
    for k, v in enumerate(table):
        total = total + v * ((n * n - (i - k) * (i - k)) // (n * n))
    return total


def greet(n, tps, me, order):
    pos = look([order.index(i) for i in range(n)], me)
    right = look(order, lax.rem(pos + 1, n))
    left = look(order, lax.rem(pos + n - 1, n))
    mine = lax.axis_index("tp")
    barrier = pltpu.get_barrier_semaphore()
    for peer in (left, right):
        pl.semaphore_signal(barrier, inc=1, device_id=(peer, mine), device_id_type=MESH)
    for k in range(1, tps):
        pl.semaphore_signal(
            barrier, inc=1, device_id=(me, lax.rem(mine + k, tps)), device_id_type=MESH
        )
    pl.semaphore_wait(barrier, 2 + tps - 1)
    return pos, right, left, mine


def remote(src, dst, send, recv, device):
    return pltpu.make_async_remote_copy(
        src_ref=src, dst_ref=dst, send_sem=send, recv_sem=recv, device_id=device, device_id_type=MESH
    )


def kernel(n, tps, picks, order, *refs):
    x_ref, meta_ref, key_hbm, value_hbm, gain_ref, out_ref = refs[:6]
    key_ref, value_ref, xall, metas, s_ref, part, got_ref, hid_ref, w_ref = refs[6:15]
    out_total, sent, came, sq_ref, sq_got = refs[15:20]
    xs, xr, ms, mr, ps, pr, ss, sr, qs, qr, kv = refs[20:]
    block, width = x_ref.shape
    half = block // 2
    experts = key_ref.shape[0]
    lines = meta_ref.shape[1] // 2
    rows = half // 2
    cuts = ss.shape[2]
    wide_out = width // cuts
    key_copy = pltpu.make_async_copy(key_hbm, key_ref, kv.at[0])
    value_copy = pltpu.make_async_copy(value_hbm, value_ref, kv.at[1])
    key_copy.start()
    me = lax.axis_index("ep")
    pos, right, left, mine = greet(n, tps, me, order)
    base = me * experts
    peers = (right, left)

    def x_copy(d, step, c, first=False):
        at = pl.ds(d * half + c * rows, rows)
        src = x_ref.at[at] if first else xall.at[step, at]
        return remote(
            src, xall.at[step + 1, at], xs.at[d, step, c], xr.at[d, step, c], (peers[d], mine)
        )

    def m_copy(d, step, first=False):
        src = meta_ref.at[d] if first else metas.at[step, d]
        return remote(src, metas.at[step + 1, d], ms.at[d, step], mr.at[d, step], (peers[d], mine))

    def p_copy(s, k):
        return remote(
            part.at[s],
            got_ref.at[s, k - 1],
            ps.at[s, k - 1],
            pr.at[s, k - 1],
            (me, lax.rem(mine + k, tps)),
        )

    for c in range(2):
        for d in (0, 1):
            x_copy(d, 0, c, True).start()
            if c == 0:
                m_copy(d, 0, True).start()
    xall[0] = x_ref[...]
    metas[0] = meta_ref[...]
    value_copy.start()
    key_copy.wait()

    per_half = LANES // picks
    sub = lax.broadcasted_iota(jnp.int32, (per_half, LANES), 0)
    lane = lax.broadcasted_iota(jnp.int32, (per_half, LANES), 1)
    own_lane = sub == lane // picks
    wide = min(512, experts)

    def pass_on(s, c):
        for d in (0, 1):
            x_copy(d, s - 1, c).wait_recv()

            @pl.when(s < n - 1)
            def _():
                x_copy(d, s, c).start()

            if c == 0:
                m_copy(d, s - 1).wait_recv()

                @pl.when(s < n - 1)
                def _():
                    m_copy(d, s).start()

    def choose(s):
        for d in (0, 1):
            all_ids = metas[s, d, :lines, :].astype(jnp.int32) - base
            for h2 in range(ROW // LANES):
                out = []
                for r in range(lines):
                    ids = all_ids[r : r + 1, h2 * LANES : (h2 + 1) * LANES]
                    ids = jnp.broadcast_to(ids, (per_half, LANES))
                    owned = (ids >= 0) & (ids < experts)
                    hi = jnp.where(owned, ids >> 7, -1)
                    lo = jnp.where(owned, ids & (LANES - 1), 0)
                    row = d * half + r * (ROW // picks) + h2 * per_half
                    acc = jnp.zeros((per_half, LANES), jnp.float32)
                    for h in range(experts // LANES):
                        tile = s_ref[row : row + per_half, h * LANES : (h + 1) * LANES]
                        acc = jnp.where(hi == h, jnp.take_along_axis(tile, lo, axis=1), acc)
                    out.append(jnp.sum(jnp.where(own_lane, acc, 0.0), axis=0, keepdims=True))
                part[s, d * lines : (d + 1) * lines, h2 * LANES : (h2 + 1) * LANES] = (
                    jnp.concatenate(out, axis=0)
                )
        for k in range(1, tps):
            p_copy(s, k).start()

    def score_step(s, carry):
        @pl.when((s >= 1) & (s < n))
        def _():
            pass_on(s, 0)

        @pl.when(s >= 1)
        def _():
            choose(s - 1)

        @pl.when((s >= 1) & (s < n))
        def _():
            pass_on(s, 1)

        @pl.when(s < n)
        def _():
            for c in range(experts // wide):
                s_ref[:, c * wide : (c + 1) * wide] = lax.dot_general(
                    xall[s],
                    key_ref[c * wide : (c + 1) * wide, :],
                    (((1,), (1,)), ((), ())),
                    preferred_element_type=jnp.float32,
                )

        return carry

    lax.fori_loop(0, n + 1, score_step, 0)
    value_copy.wait()

    per = ROW // picks
    tall = experts // ROW * per
    lane_token = lax.broadcasted_iota(jnp.int32, (lines, ROW), 1) // picks
    tall_iota = lax.broadcasted_iota(jnp.int32, (tall, ROW), 0)
    lo_iota = lax.broadcasted_iota(jnp.int32, (ROW, ROW), 0)

    def copy(d, s, c):
        return remote(
            sent.at[s, d, c], came.at[s, d, c], ss.at[d, s, c], sr.at[d, s, c], (peers[d], mine)
        )

    def mix_step(s, carry):
        slot = lax.rem(s + 1, n)
        total = part[slot]
        for k in range(1, tps):
            p_copy(slot, k).wait()
            total = total + got_ref[slot, k - 1]
        hid_ref[...] = 0.5 * total * (1.0 + lax.erf(total * (0.5**0.5)))
        for d in (0, 1):
            ids = metas[slot, d, :lines, :].astype(jnp.int32) - base
            owned = (ids >= 0) & (ids < experts)
            codes = jnp.where(owned, (ids >> 8) * per + lane_token, -1)
            los = ids & (ROW - 1)
            hs = hid_ref[d * lines : (d + 1) * lines, :] * metas[slot, d, lines:, :]
            for r in range(lines):
                code, lo, h = codes[r : r + 1, :], los[r : r + 1, :], hs[r : r + 1, :]
                a = jnp.where(tall_iota == code, h, 0.0).astype(jnp.bfloat16)
                b = jnp.where(lo_iota == lo, 1.0, 0.0).astype(jnp.bfloat16)
                w = lax.dot_general(
                    a, b, (((1,), (1,)), ((), ())), preferred_element_type=jnp.float32
                ).astype(jnp.bfloat16)
                row = d * half + r * per
                for c in range(experts // ROW):
                    w_ref[row : row + per, c * ROW : (c + 1) * ROW] = w[c * per : (c + 1) * per, :]
        for c in range(cuts):
            cols = slice(c * wide_out, (c + 1) * wide_out)
            out_total[:, cols] = jnp.dot(
                w_ref[...], value_ref[:, cols], preferred_element_type=jnp.float32
            )
            for d in (0, 1):
                at = slice(d * half, (d + 1) * half)

                @pl.when(s >= 1)
                def _():
                    copy(d, s - 1, c).wait_recv()
                    out_total[at, cols] = out_total[at, cols] + came[s - 1, d, c].astype(
                        jnp.float32
                    )

                @pl.when(s < n - 1)
                def _():
                    sent[s, d, c] = out_total[at, cols].astype(jnp.bfloat16)
                    copy(d, s, c).start()

        return carry

    lax.fori_loop(0, n, mix_step, 0)
    mixed = out_total[...]
    ones = jnp.ones((8, width), jnp.float32)
    square = lax.dot_general(
        ones,
        mixed * mixed,
        (((1,), (1,)), ((), ())),
        precision=lax.Precision.HIGHEST,
        preferred_element_type=jnp.float32,
    )
    sq_ref[...] = square

    def q_copy(k):
        return remote(
            sq_ref, sq_got.at[k - 1], qs.at[k - 1], qr.at[k - 1], (me, lax.rem(mine + k, tps))
        )

    for k in range(1, tps):
        q_copy(k).start()

    def drain(s, carry):
        for d in (0, 1):
            m_copy(d, s).wait_send()
            for c in range(2):
                x_copy(d, s, c).wait_send()
            for c in range(cuts):
                copy(d, s, c).wait_send()
        return carry

    lax.fori_loop(0, n - 1, drain, 0)
    for k in range(1, tps):
        q_copy(k).wait()
    total = square
    for k in range(1, tps):
        total = total + sq_got[k - 1]
    scale = lax.rsqrt(total / (width * tps) + 1e-06)
    column = lax.dot_general(
        scale,
        jnp.full((8, LANES), 0.125, jnp.float32),
        (((0,), (0,)), ((), ())),
        precision=lax.Precision.HIGHEST,
        preferred_element_type=jnp.float32,
    )
    for c in range(width // LANES):
        at = slice(c * LANES, (c + 1) * LANES)
        out_ref[:, at] = (out_total[:, at] * column * gain_ref[:, at]).astype(jnp.bfloat16)


def body(tokens, row_ids, row_gates, key_table, value_table, norm_gain):
    block, width = tokens.shape
    picks = row_ids.shape[1]
    experts = key_table.shape[0]
    n, tps = lax.axis_size("ep"), lax.axis_size("tp")
    half = block // 2
    lines = half * picks // ROW
    cuts = 2 if width % (2 * LANES) == 0 else 1
    meta = jnp.concatenate(
        [
            row_ids.astype(jnp.float32).reshape(2, lines, ROW),
            row_gates.reshape(2, lines, ROW),
        ],
        axis=1,
    )
    whole = pl.BlockSpec(memory_space=pltpu.VMEM)
    hbm = pl.BlockSpec(memory_space=pl.ANY)
    dma = pltpu.SemaphoreType.DMA
    bf16, f32 = jnp.bfloat16, jnp.float32
    return pl.pallas_call(
        functools.partial(kernel, n, tps, picks, cycle_of(n)),
        out_shape=jax.ShapeDtypeStruct((block, width), bf16),
        in_specs=[whole, whole, hbm, hbm, whole],
        out_specs=whole,
        scratch_shapes=[
            pltpu.VMEM((experts, width), bf16),
            pltpu.VMEM((experts, width), bf16),
            pltpu.VMEM((n, block, width), bf16),
            pltpu.VMEM((n, 2, 2 * lines, ROW), f32),
            pltpu.VMEM((block, experts), f32),
            pltpu.VMEM((n, 2 * lines, ROW), f32),
            pltpu.VMEM((n, tps - 1, 2 * lines, ROW), f32),
            pltpu.VMEM((2 * lines, ROW), f32),
            pltpu.VMEM((block, experts), bf16),
            pltpu.VMEM((block, width), f32),
            pltpu.VMEM((n - 1, 2, cuts, half, width // cuts), bf16),
            pltpu.VMEM((n - 1, 2, cuts, half, width // cuts), bf16),
            pltpu.VMEM((8, block), f32),
            pltpu.VMEM((tps - 1, 8, block), f32),
            dma((2, n - 1, 2)),
            dma((2, n - 1, 2)),
            dma((2, n - 1)),
            dma((2, n - 1)),
            dma((n, tps - 1)),
            dma((n, tps - 1)),
            dma((2, n - 1, cuts)),
            dma((2, n - 1, cuts)),
            dma((tps - 1,)),
            dma((tps - 1,)),
            dma((2,)),
        ],
        compiler_params=pltpu.CompilerParams(collective_id=0, has_side_effects=True),
    )(tokens, meta, key_table, value_table, norm_gain.reshape(1, -1))


def solution(mesh):
    in_specs = (P("ep", "tp"), P("ep", None), P("ep", None), P("ep", "tp"), P("ep", "tp"), P("tp"))
    out_specs = P("ep", "tp")
    return jax.shard_map(body, mesh=mesh, in_specs=in_specs, out_specs=out_specs, check_vma=False)
```

time: 90.5 us -> 75.5 us (0.83)
  Pallas kernels: 86 us -> 71 us
    pallas_call x2 -> x1, Pallas kernels: 86 us -> 71 us  [body(): pl.pallas_call(functools.partial(kernel, n, tps, picks, cycle_of(n)), out...]
where the time goes in v2:
time: 75.5 us; the launch traced here: 75.1 us
  Pallas kernels  71 us (94%)
  local copies, waits for them, and re-layouts  2.81 us (4%)
  other arithmetic  1.34 us (2%)
    pallas_call x1, Pallas kernels, body(): pl.pallas_call(functools.partial(kernel, n, tps, picks, cycle_of(n)), out...  71 us
    unnamed x2, local copies, waits for them, and re-layouts  2.49 us

profile of v2, /device:TPU:0, one launch (start us, length us, event | category | flops | bytes accessed | tf_op | source)
XLA Modules:
  0.0 75.1 jit_solution(12791510419693067018)
XLA Ops:
  0.0 0.7 convert_element_type.3
  0.7 0.1 copy.9
  0.8 0.1 reshape.9
  0.9 0.8 %copy.10 = f32[256,16]{1,0:T(8,128)S(1)} copy(f32[256,16]{0,1:T(8,128)} %param.8) | data formatting | bytes 32768 | tf_op args[2]
  1.8 0.1 reshape.10
  1.9 0.6 pad_maximum_fusion.refs_1_
  2.5 71.0 %shard_map.64 = bf16[256,512]{1,0:T(8,128)(2,1)} custom-call(bf16[256,512]{1,0:T(8,128)(2,1)} %refs_0_.1, f32[2,16,256]{2,1,0:T(8,128)} %pad_maximum_fusion.refs_1_, bf16[4096,512]{1,0:T(8,128)(2,1)} %refs_2_.1, bf16[4096,512]{1,0:T(8,128)(2,1)} %refs_3_.1, f32[1,512]{1,0:T(1,128)} %bitcast.1), custom_call_target="tpu_custom_call" | custom-call | tf_op jit(solution)/shard_map/pallas_call | solution.py:304
  73.5 1.7 %copy.12 = bf16[256,512]{1,0:T(8,128)(2,1)} copy(bf16[256,512]{1,0:T(8,128)(2,1)} %shard_map.64) | data formatting | bytes 524288
